TPU v7x, 32 devices: a whole 2x2x4 slice. The times are simulated.
32 devices in a mesh: grp: 2 (over y), fs: 4 (over z), tp: 4 (over x, core).
Axes of the slice: x: 2, y: 2, z: 4, core: 2. Of those that a mesh axis runs over, the one named last changes fastest.
Arguments:
- tokens: bfloat16 [2048, 2048], P(('grp', 'fs'), 'tp'), parts along dimension 0, may hold values from -6 to 6
- recurrent_norm_gain: float32 [2048], replicated, may hold values from 0.1 to 1.9
- feedforward_norm_gain: float32 [2048], replicated, may hold values from 0.1 to 1.9
- gate_projection_weight: bfloat16 [2048, 2048], P('fs', 'tp'), may hold values from -0.125 to 0.125
- recurrent_projection_weight: bfloat16 [2048, 2048], P('fs', 'tp'), may hold values from -0.125 to 0.125
- convolution_kernel: bfloat16 [4, 2048], P(None, 'tp'), may hold values from -3 to 3
- decay_gate_matrix: bfloat16 [16, 128, 128], P('tp'), may hold values from -0.5 to 0.5
- input_gate_matrix: bfloat16 [16, 128, 128], P('tp'), may hold values from -0.5 to 0.5
- base_decay_logit: float32 [2048], P('tp'), may hold values from 3 to 9
- extra_log_decay: float32 [2048], P(('grp', 'fs')), parts along dimension 0, may hold values from -0.7 to 0
- output_projection_weight: bfloat16 [2048, 2048], P('tp', 'fs'), may hold values from -0.125 to 0.125
- up_projection_weight: bfloat16 [2048, 8192], P('fs', 'tp'), may hold values from -0.125 to 0.125
- down_projection_weight: bfloat16 [8192, 2048], P('tp', 'fs'), may hold values from -0.0625 to 0.0625
Outputs:
- layer_out: bfloat16 [2048, 2048], P(('grp', 'fs'), 'tp'), parts along dimension 0
There are 2 independent parts, one for each index of `grp`. A program takes and returns all parts, laid end to end along the dimension named above; an argument that names none is the same for every part. Nothing has to cross between parts.
All inputs are finite; a program needn't handle non-finite values.
Results may differ from a plain program's by a relative error of at most 0.018.
Values may be sent and summed in bfloat16 or wider, within the bound.
A program may use at most 64 MiB of HBM per device.

v0:
```python
import jax
import jax.numpy as jnp
from jax import lax
from jax.sharding import PartitionSpec as P


def rms_rows(values_in, norm_gain):
    values = values_in.astype(jnp.float32)
    inverse = lax.rsqrt(jnp.mean(values * values, axis=-1, keepdims=True) + 1e-06)
    return (values * inverse * norm_gain).astype(jnp.bfloat16)


def combine(earlier, later):
    return (earlier[0] * later[0], later[0] * earlier[1] + later[1])


def recurrent_state(
    recurrent_branch_rows,
    gate_branch_rows,
    convolution_kernel,
    decay_gate_matrix,
    input_gate_matrix,
    base_decay_logit,
    extra_log_decay,
):
    length = recurrent_branch_rows.shape[0]
    taps = convolution_kernel.shape[0]
    padded = jnp.pad(recurrent_branch_rows.astype(jnp.float32), ((taps - 1, 0), (0, 0)))
    conv_sum = jnp.zeros((length, recurrent_branch_rows.shape[1]), jnp.float32)
    for tap_index in range(taps):
        conv_sum = conv_sum + padded[tap_index : tap_index + length] * convolution_kernel[
            tap_index
        ].astype(jnp.float32)
    conv_rows = conv_sum.astype(jnp.bfloat16)
    blocks = decay_gate_matrix.shape[0]
    blocked = conv_rows.reshape(length, blocks, -1)
    recurrence_gate = jax.nn.sigmoid(
        jnp.einsum(
            "tni,nij->tnj", blocked, decay_gate_matrix, preferred_element_type=jnp.float32
        ).reshape(length, -1)
    )
    input_rate = jax.nn.sigmoid(
        jnp.einsum(
            "tni,nij->tnj", blocked, input_gate_matrix, preferred_element_type=jnp.float32
        ).reshape(length, -1)
    )
    decay_log_values = (
        -8.0 * jax.nn.softplus(-base_decay_logit) * recurrence_gate + extra_log_decay[:, None]
    )
    decay = jnp.exp(decay_log_values)
    drive = (
        jnp.sqrt(-jnp.expm1(2.0 * decay_log_values)) * input_rate * conv_rows.astype(jnp.float32)
    )
    _, hidden = lax.associative_scan(combine, (decay, drive), axis=0)
    return (hidden * gate_branch_rows.astype(jnp.float32)).astype(jnp.bfloat16)


def per_device(
    tokens,
    recurrent_norm_gain,
    feedforward_norm_gain,
    gate_projection_weight,
    recurrent_projection_weight,
    convolution_kernel,
    decay_gate_matrix,
    input_gate_matrix,
    base_decay_logit,
    extra_log_decay,
    output_projection_weight,
    up_projection_weight,
    down_projection_weight,
):
    whole_rows = lax.all_gather(tokens, "tp", axis=1, tiled=True)
    normed = rms_rows(whole_rows, recurrent_norm_gain)
    columns = normed
    gate_pre = jnp.dot(
        columns,
        lax.all_gather(gate_projection_weight, "fs", axis=0, tiled=True),
        preferred_element_type=jnp.float32,
    )
    recur_pre = jnp.dot(
        columns,
        lax.all_gather(recurrent_projection_weight, "fs", axis=0, tiled=True),
        preferred_element_type=jnp.float32,
    )
    gate_branch_rows = jax.nn.gelu(gate_pre).astype(jnp.bfloat16)
    recurrent_branch_rows = recur_pre.astype(jnp.bfloat16)
    mixed_output = recurrent_state(
        recurrent_branch_rows,
        gate_branch_rows,
        convolution_kernel,
        decay_gate_matrix,
        input_gate_matrix,
        base_decay_logit,
        extra_log_decay,
    )
    partials = jnp.dot(
        mixed_output,
        lax.all_gather(output_projection_weight, "fs", axis=1, tiled=True),
        preferred_element_type=jnp.float32,
    )
    residual = (
        tokens.astype(jnp.float32)
        + lax.psum_scatter(
            partials.astype(jnp.bfloat16), "tp", scatter_dimension=1, tiled=True
        ).astype(jnp.float32)
    ).astype(jnp.bfloat16)
    middle = lax.all_gather(residual, "tp", axis=1, tiled=True)
    channel_in = rms_rows(middle, feedforward_norm_gain)
    columns = channel_in
    upward = jnp.dot(
        columns,
        lax.all_gather(up_projection_weight, "fs", axis=0, tiled=True),
        preferred_element_type=jnp.float32,
    )
    positive = jnp.maximum(upward, 0.0)
    squared = (positive * positive).astype(jnp.bfloat16)
    down_terms = jnp.dot(
        squared,
        lax.all_gather(down_projection_weight, "fs", axis=1, tiled=True),
        preferred_element_type=jnp.float32,
    )
    summed_down = lax.psum_scatter(
        down_terms.astype(jnp.bfloat16), "tp", scatter_dimension=1, tiled=True
    ).astype(jnp.float32)
    return (residual.astype(jnp.float32) + summed_down).astype(jnp.bfloat16)


def solution(mesh):
    placed = (
        P(("grp", "fs"), "tp"),
        P(),
        P(),
        P("fs", "tp"),
        P("fs", "tp"),
        P(None, "tp"),
        P("tp", None, None),
        P("tp", None, None),
        P("tp"),
        P(("grp", "fs")),
        P("tp", "fs"),
        P("fs", "tp"),
        P("tp", "fs"),
    )
    return jax.shard_map(
        per_device, mesh=mesh, in_specs=placed, out_specs=P(("grp", "fs"), "tp"), check_vma=False
    )
```

profile of v0, /device:TPU:0, one launch (start us, length us, event | category | flops | bytes accessed | tf_op | source)
XLA Modules:
  0.0 558.3 jit_solution(17213416898491841167)
XLA Ops:
  6.5 0.7 all-gather.8.cloned.1.call-update
  7.3 0.7 all-gather.10.cloned.1.call-update
  8.1 0.7 all-gather.12.cloned.1.call-update
  9.4 0.8 slice_convert_fusion.3
  10.2 0.7 fusion.55
  10.9 17.4 %all-gather.8.cloned.1.call-done = bf16[256,2048]{1,0:T(8,128)(2,1)} async-done(((bf16[256,512]{1,0:T(8,128)(2,1)}), bf16[256,2048]{1,0:T(8,128)(2,1)}) %all-gather.8.cloned.1.call-update) | async-done | bytes 1048592 | tf_op jit(solution)/shard_map/all_gather | solution.py:73
  28.4 1.5 fusion.2
  29.9 45.7 %all-gather.10.cloned.1.call-done = bf16[2048,512]{1,0:T(8,128)(2,1)} async-done(((bf16[512,512]{1,0:T(8,128)(2,1)}), bf16[2048,512]{1,0:T(8,128)(2,1)}) %all-gather.10.cloned.1.call-update) | async-done | bytes 2097168 | tf_op jit(solution)/shard_map/all_gather | solution.py:83
  75.6 2.7 fusion.14
  79.8 0.7 fusion.29
  85.2 36.4 %all-gather.12.cloned.1.call-done = bf16[2048,512]{1,0:T(8,128)(2,1)} async-done(((bf16[512,512]{1,0:T(8,128)(2,1)}), bf16[2048,512]{1,0:T(8,128)(2,1)}) %all-gather.12.cloned.1.call-update) | async-done | bytes 2097168 | tf_op jit(solution)/shard_map/all_gather | solution.py:78
  121.7 45.9 %all-gather.14.cloned.1.call-done = bf16[512,2048]{1,0:T(8,128)(2,1)} async-done(((bf16[512,512]{1,0:T(8,128)(2,1)}), bf16[512,2048]{1,0:T(8,128)(2,1)}) %all-gather.14.cloned.1.call-update) | async-done | bytes 2097168 | tf_op jit(solution)/shard_map/all_gather | solution.py:99
  167.6 4.8 convolution_convert_fusion
  172.5 23.7 %reduce-scatter.3.cloned.1.call-done = bf16[256,512]{1,0:T(8,128)(2,1)} async-done(((bf16[256,2048]{1,0:T(8,128)(2,1)}), bf16[256,512]{1,0:T(8,128)(2,1)}) %reduce-scatter.3.cloned.1.call-update) | async-done | bytes 262160 | tf_op jit(solution)/shard_map/reduce_scatter | solution.py:104
  196.1 1.7 add_convert_fusion.1
  197.9 0.7 all-gather.18.cloned.1.call-update
  198.7 0.7 all-gather.20.cloned.1.call-update
  199.4 15.3 %all-gather.16.cloned.1.call-done = bf16[256,2048]{1,0:T(8,128)(2,1)} async-done(((bf16[256,512]{1,0:T(8,128)(2,1)}), bf16[256,2048]{1,0:T(8,128)(2,1)}) %all-gather.16.cloned.1.call-update) | async-done | bytes 1048592 | tf_op jit(solution)/shard_map/all_gather | solution.py:108
  214.7 1.5 fusion.5
  216.3 149.7 %all-gather.18.cloned.1.call-done = bf16[2048,2048]{1,0:T(8,128)(2,1)} async-done(((bf16[512,2048]{1,0:T(8,128)(2,1)}), bf16[2048,2048]{1,0:T(8,128)(2,1)}) %all-gather.18.cloned.1.call-update) | async-done | bytes 8388624 | tf_op jit(solution)/shard_map/all_gather | solution.py:113
  366.0 149.4 %all-gather.20.cloned.1.call-done = bf16[2048,2048]{1,0:T(8,128)(2,1)} async-done(((bf16[2048,512]{1,0:T(8,128)(2,1)}), bf16[2048,2048]{1,0:T(8,128)(2,1)}) %all-gather.20.cloned.1.call-update) | async-done | bytes 8388624 | tf_op jit(solution)/shard_map/all_gather | solution.py:120
  515.4 11.6 %convolution_convert_fusion.1 = bf16[256,2048]{1,0:T(8,128)(2,1)} fusion(bf16[2048,2048]{1,0:T(8,128)(2,1)} %all-gather.20.cloned.1.call-done, bf16[2048,2048]{1,0:T(8,128)(2,1)} %all-gather.18.cloned.1.call-done, bf16[256,2048]{1,0:T(8,128)(2,1)} %all-gather.16.cloned.1.call-done, f32[2048]{0:T(1024)S(1)} %copy-done.7, f32[256]{0:T(256)S(1)} %add_rsqrt_fusion), kind=kOutput, calls=%fused_computation.8 | convolution fusion | flops 4299161600 | bytes 18883584 | tf_op jit(solution)/shard_map/dot_general | solution.py:118
  527.0 23.1 %reduce-scatter.5.cloned.1.call-done = bf16[256,512]{1,0:T(8,128)(2,1)} async-done(((bf16[256,2048]{1,0:T(8,128)(2,1)}), bf16[256,512]{1,0:T(8,128)(2,1)}) %reduce-scatter.5.cloned.1.call-update) | async-done | bytes 262160 | tf_op jit(solution)/shard_map/reduce_scatter | solution.py:123
  550.1 1.7 add_convert_fusion
  (125 shorter events, 6.7 us)
Async XLA Ops:
  6.5 72.0 %copy-start = (bf16[4,128,128]{2,1,0:T(8,128)(2,1)S(1)}, bf16[4,128,128]{2,1,0:T(8,128)(2,1)}, u32[]{:S(2)}) copy-start(bf16[4,128,128]{2,1,0:T(8,128)(2,1)} %param.19) | copy-start | bytes 393220
  6.5 69.1 %copy-start.6 = (f32[2048]{0:T(1024)S(1)}, f32[2048]{0:T(1024)}, u32[]{:S(2)}) copy-start(f32[2048]{0:T(1024)} %param.14) | copy-start | bytes 24580
  6.5 21.8 %all-gather.8.cloned.1.call-start = ((), (), s32[]{:S(2)}) async-start(), calls=%async_computation.2 | async-start | bytes 1310720 | tf_op jit(solution)/shard_map/all_gather | solution.py:73
  7.3 68.3 %all-gather.10.cloned.1.call-start = ((), (), s32[]{:S(2)}) async-start(), calls=%async_computation.3 | async-start | bytes 2621440 | tf_op jit(solution)/shard_map/all_gather | solution.py:83
  8.0 113.7 %all-gather.12.cloned.1.call-start = ((), (), s32[]{:S(2)}) async-start(), calls=%async_computation.4 | async-start | bytes 2621440 | tf_op jit(solution)/shard_map/all_gather | solution.py:78
  8.7 158.9 %all-gather.14.cloned.1.call-start = ((), (), s32[]{:S(2)}) async-start(), calls=%async_computation.5 | async-start | bytes 2621440 | tf_op jit(solution)/shard_map/all_gather | solution.py:99
  9.3 186.8 %reduce-scatter.3.cloned.1.call-start = ((), (), s32[]{:S(2)}) async-start(), calls=%async_computation.6 | async-start | bytes 1310720 | tf_op jit(solution)/shard_map/reduce_scatter | solution.py:104
  78.3 0.9 copy-start.5
  78.9 0.8 copy-start.4
  84.9 82.7 %copy-start.3 = (bf16[256,2048]{1,0:T(8,128)(2,1)S(1)}, bf16[256,2048]{1,0:T(8,128)(2,1)}, u32[]{:S(2)}) copy-start(bf16[256,2048]{1,0:T(8,128)(2,1)} %all-gather.8.cloned.1.call-done) | copy-start | bytes 3145732
  85.2 110.9 %copy-start.2 = (bf16[256,512]{1,0:T(8,128)(2,1)S(1)}, bf16[256,512]{1,0:T(8,128)(2,1)}, u32[]{:S(2)}) copy-start(bf16[256,512]{1,0:T(8,128)(2,1)} %param.13) | copy-start | bytes 786436
  172.4 42.3 %all-gather.16.cloned.1.call-start = ((), (), s32[]{:S(2)}) async-start(), calls=%async_computation.7 | async-start | bytes 1310720 | tf_op jit(solution)/shard_map/all_gather | solution.py:108
  197.9 168.1 %all-gather.18.cloned.1.call-start = ((), (), s32[]{:S(2)}) async-start(), calls=%async_computation.8 | async-start | bytes 10485760 | tf_op jit(solution)/shard_map/all_gather | solution.py:113
  198.6 316.7 %copy-start.7 = (f32[2048]{0:T(1024)S(1)}, f32[2048]{0:T(1024)}, u32[]{:S(2)}) copy-start(f32[2048]{0:T(1024)} %param.15) | copy-start | bytes 24580
  198.6 316.7 %all-gather.20.cloned.1.call-start = ((), (), s32[]{:S(2)}) async-start(), calls=%async_computation.9 | async-start | bytes 10485760 | tf_op jit(solution)/shard_map/all_gather | solution.py:120
  199.4 350.7 %reduce-scatter.5.cloned.1.call-start = ((), (), s32[]{:S(2)}) async-start(), calls=%async_computation.10 | async-start | bytes 1310720 | tf_op jit(solution)/shard_map/reduce_scatter | solution.py:123
  216.3 333.8 %copy-start.1 = (bf16[256,512]{1,0:T(8,128)(2,1)S(1)}, bf16[256,512]{1,0:T(8,128)(2,1)}, u32[]{:S(2)}) copy-start(bf16[256,512]{1,0:T(8,128)(2,1)} %add_convert_fusion.1) | copy-start | bytes 786436
Sparse Core Ops, SparseCore 0:
  8.9 19.4 all-gather.7
  29.9 45.6 all-gather.9
  77.2 44.4 all-gather.11
  123.1 44.4 all-gather.13
  172.5 23.5 reduce-scatter.2
  198.0 16.6 all-gather.15
  216.3 149.6 all-gather.17
  367.5 147.7 all-gather.19
  527.1 22.9 reduce-scatter.4
where the time goes:
time: 559 us; the launch traced here: 558 us
  waiting for transfers between devices  511 us (91%)
  matrix products  19.7 us (4%)
  between operations  13.8 us (2%)
  other arithmetic  9.49 us (2%)
    all_gather x1, waiting for transfers between devices, per_device(): lax.all_gather(up_projection_weight, 'fs', axis=0, tiled=True)  150 us
    all_gather x1, waiting for transfers between devices, per_device(): lax.all_gather(down_projection_weight, 'fs', axis=1, tiled=True)  149 us
    all_gather x1, waiting for transfers between devices, per_device(): lax.all_gather(output_projection_weight, 'fs', axis=1, tiled=True)  45.9 us
    all_gather x1, waiting for transfers between devices, per_device(): lax.all_gather(recurrent_projection_weight, 'fs', axis=0, tiled=True)  45.7 us
    all_gather x1, waiting for transfers between devices, per_device(): lax.all_gather(gate_projection_weight, 'fs', axis=0, tiled=True)  36.4 us
    reduce_scatter x1, waiting for transfers between devices, per_device(): lax.psum_scatter(partials.astype(jnp.bfloat16), 'tp', scatter_dimension=1...  23.7 us
    reduce_scatter x1, waiting for transfers between devices, per_device(): lax.psum_scatter(down_terms.astype(jnp.bfloat16), 'tp', scatter_dimension...  23.1 us
    all_gather x1, waiting for transfers between devices, per_device(): whole_rows = lax.all_gather(tokens, 'tp', axis=1, tiled=True)  17.4 us
  transfers between devices with their start and end apart: 9, of which 9 were waited for; matrix products, arithmetic and copies ran while one was open for 2% of the time, Pallas kernels for 0%

commit v1 on v0

--- a/solution.py
+++ b/solution.py
@@ -108,10 +108,44 @@
     middle = lax.all_gather(residual, "tp", axis=1, tiled=True)
     channel_in = rms_rows(middle, feedforward_norm_gain)
     columns = channel_in
+
+    def numbers_post(payload, axis_key="fs"):
+        big = lax.axis_size(axis_key)
+        view_out, e_now, x_next = (big, lax.axis_index(axis_key), payload.shape[0])
+        step_out = lax.dynamic_update_slice_in_dim(
+            jnp.zeros(
+                [q * view_out if to_i == 0 else q for to_i, q in enumerate(payload.shape)],
+                payload.dtype,
+            ),
+            payload,
+            e_now * x_next,
+            axis=0,
+        )
+        rr = 1
+        taken_in = val2 = payload
+        while rr < view_out // 2 + 1:
+            taken_in = lax.ppermute(
+                taken_in,
+                axis_name=axis_key,
+                perm=[(to_i, (to_i + 1) % view_out) for to_i in range(view_out)],
+            )
+            step_out = lax.dynamic_update_slice_in_dim(
+                step_out, taken_in, (e_now - rr) % view_out * x_next, axis=0
+            )
+            if 2 * rr < view_out:
+                val2 = lax.ppermute(
+                    val2,
+                    axis_name=axis_key,
+                    perm=[(to_i, (to_i - 1) % view_out) for to_i in range(view_out)],
+                )
+                step_out = lax.dynamic_update_slice_in_dim(
+                    step_out, val2, (e_now + rr) % view_out * x_next, axis=0
+                )
+            rr += 1
+        return step_out
+
     upward = jnp.dot(
-        columns,
-        lax.all_gather(up_projection_weight, "fs", axis=0, tiled=True),
-        preferred_element_type=jnp.float32,
+        columns, numbers_post(up_projection_weight), preferred_element_type=jnp.float32
     )
     positive = jnp.maximum(upward, 0.0)
     squared = (positive * positive).astype(jnp.bfloat16)

time: 559 us -> 518 us (0.927)
  waiting for transfers between devices: 511 us -> 407 us
  starting transfers between devices: 0.31 us -> 47.8 us
  local copies, waits for them, and re-layouts: 4.25 us -> 19.6 us
    ppermute x0 -> x3, waiting for transfers between devices: none -> 188 us  [the longest x2 101 us: numbers_post(): lax.ppermute(taken_in, axis_name=axis_key, perm=[(to_i, (to_i + 1) % view...]
    all_gather x1 -> x0, waiting for transfers between devices: 150 us -> none  [per_device(): lax.all_gather(up_projection_weight, 'fs', axis=0, tiled=True)]
    all_gather x1, waiting for transfers between devices: 149 us -> 21.8 us  [per_device(): lax.all_gather(down_projection_weight, 'fs', axis=1, tiled=True)]
    ppermute x0 -> x3, starting transfers between devices: none -> 47.5 us  [the longest x2 45.1 us: numbers_post(): lax.ppermute(taken_in, axis_name=axis_key, perm=[(to_i, (to_i + 1) % view...]
    all_gather x1, waiting for transfers between devices: 15.3 us -> 0.01 us  [per_device(): middle = lax.all_gather(residual, 'tp', axis=1, tiled=True)]
    dynamic_update_slice x0 -> x4, local copies, waits for them, and re-layouts: none -> 11 us  [the longest x2 6.33 us: numbers_post(): lax.dynamic_update_slice_in_dim(step_out, taken_in, (e_now - rr) % view_o...]
  transfers between devices with their start and end apart: 9 -> 11, of which waited for: 9 -> 10; matrix products, arithmetic and copies ran while one was open for 2% -> 6% of each run, Pallas kernels for 0% -> 0%
where the time goes in v1:
time: 518 us
  waiting for transfers between devices  407 us (79%)
  starting transfers between devices  47.8 us (9%)
  matrix products  19.8 us (4%)
  local copies, waits for them, and re-layouts  19.6 us (4%)
  between operations  14.1 us (3%)
  other arithmetic  9.49 us (2%)
    ppermute x2, waiting for transfers between devices, numbers_post(): lax.ppermute(taken_in, axis_name=axis_key, perm=[(to_i, (to_i + 1) % view...  101 us
    ppermute x1, waiting for transfers between devices, numbers_post(): lax.ppermute(val2, axis_name=axis_key, perm=[(to_i, (to_i - 1) % view_out...  87 us
    all_gather x1, waiting for transfers between devices, per_device(): lax.all_gather(output_projection_weight, 'fs', axis=1, tiled=True)  45.9 us
    all_gather x1, waiting for transfers between devices, per_device(): lax.all_gather(recurrent_projection_weight, 'fs', axis=0, tiled=True)  45.7 us
    ppermute x2, starting transfers between devices, numbers_post(): lax.ppermute(taken_in, axis_name=axis_key, perm=[(to_i, (to_i + 1) % view...  45.1 us
    all_gather x1, waiting for transfers between devices, per_device(): lax.all_gather(gate_projection_weight, 'fs', axis=0, tiled=True)  36.4 us
    reduce_scatter x1, waiting for transfers between devices, per_device(): lax.psum_scatter(down_terms.astype(jnp.bfloat16), 'tp', scatter_dimension...  24.7 us
    reduce_scatter x1, waiting for transfers between devices, per_device(): lax.psum_scatter(partials.astype(jnp.bfloat16), 'tp', scatter_dimension=1...  23.7 us
  transfers between devices with their start and end apart: 11, of which 10 were waited for; matrix products, arithmetic and copies ran while one was open for 6% of the time, Pallas kernels for 0%

profile of v1, /device:TPU:0, one launch (start us, length us, event | category | flops | bytes accessed | tf_op | source)
XLA Modules:
  0.0 517.7 jit_solution(7174164210562795546)
XLA Ops:
  10.9 17.4 %all-gather.7.cloned.1.call-done = bf16[256,2048]{1,0:T(8,128)(2,1)} async-done(((bf16[256,512]{1,0:T(8,128)(2,1)}), bf16[256,2048]{1,0:T(8,128)(2,1)}) %all-gather.7.cloned.1.call-update) | async-done | bytes 1048592 | tf_op jit(solution)/shard_map/all_gather | solution.py:73
  28.4 1.5 fusion.2
  29.9 45.7 %all-gather.9.cloned.1.call-done = bf16[2048,512]{1,0:T(8,128)(2,1)} async-done(((bf16[512,512]{1,0:T(8,128)(2,1)}), bf16[2048,512]{1,0:T(8,128)(2,1)}) %all-gather.9.cloned.1.call-update) | async-done | bytes 2097168 | tf_op jit(solution)/shard_map/all_gather | solution.py:83
  75.6 2.7 fusion.14
  85.2 36.4 %all-gather.11.cloned.1.call-done = bf16[2048,512]{1,0:T(8,128)(2,1)} async-done(((bf16[512,512]{1,0:T(8,128)(2,1)}), bf16[2048,512]{1,0:T(8,128)(2,1)}) %all-gather.11.cloned.1.call-update) | async-done | bytes 2097168 | tf_op jit(solution)/shard_map/all_gather | solution.py:78
  121.7 45.9 %all-gather.13.cloned.1.call-done = bf16[512,2048]{1,0:T(8,128)(2,1)} async-done(((bf16[512,512]{1,0:T(8,128)(2,1)}), bf16[512,2048]{1,0:T(8,128)(2,1)}) %all-gather.13.cloned.1.call-update) | async-done | bytes 2097168 | tf_op jit(solution)/shard_map/all_gather | solution.py:99
  167.6 4.8 convolution_convert_fusion
  172.5 23.7 %reduce-scatter.3.cloned.1.call-done = bf16[256,512]{1,0:T(8,128)(2,1)} async-done(((bf16[256,2048]{1,0:T(8,128)(2,1)}), bf16[256,512]{1,0:T(8,128)(2,1)}) %reduce-scatter.3.cloned.1.call-update) | async-done | bytes 262160 | tf_op jit(solution)/shard_map/reduce_scatter | solution.py:104
  196.2 1.7 add_convert_fusion.1
  198.7 1.5 collective-permute-start
  200.3 2.3 collective-permute-start.1
  202.6 65.4 %collective-permute-done = bf16[512,2048]{1,0:T(8,128)(2,1)} collective-permute-done((bf16[512,2048]{1,0:T(8,128)(2,1)S(1)}, bf16[512,2048]{1,0:T(8,128)(2,1)}, u32[]{:S(2)}, u32[]{:S(2)}) %collective-permute-start) | collective-permute-done | bytes 2097184 | tf_op jit(solution)/shard_map/ppermute | solution.py:127
  268.0 43.6 %collective-permute-start.2 = (bf16[512,2048]{1,0:T(8,128)(2,1)}, bf16[512,2048]{1,0:T(8,128)(2,1)}, u32[]{:S(2)}, u32[]{:S(2)}) collective-permute-start(bf16[512,2048]{1,0:T(8,128)(2,1)} %collective-permute-done), channel_id=1, source_target_pairs={{0,4},{4,8},{8,12},{12,0},{1,5},{5,9},{9,13},{13,1},{2,6},{6,10},{... | collective-permute-start | bytes 6291464 | tf_op jit(solution)/shard_map/ppermute | solution.py:127
  311.6 4.3 broadcast_in_dim.2
  317.4 3.2 constant_dynamic-update-slice_fusion.2
  320.6 87.0 %collective-permute-done.1 = bf16[512,2048]{1,0:T(8,128)(2,1)} collective-permute-done((bf16[512,2048]{1,0:T(8,128)(2,1)S(1)}, bf16[512,2048]{1,0:T(8,128)(2,1)}, u32[]{:S(2)}, u32[]{:S(2)}) %collective-permute-start.1) | collective-permute-done | bytes 2097184 | tf_op jit(solution)/shard_map/ppermute | solution.py:136
  407.6 3.2 constant_dynamic-update-slice_fusion.1
  410.8 35.7 %collective-permute-done.2 = bf16[512,2048]{1,0:T(8,128)(2,1)} collective-permute-done((bf16[512,2048]{1,0:T(8,128)(2,1)}, bf16[512,2048]{1,0:T(8,128)(2,1)}, u32[]{:S(2)}, u32[]{:S(2)}) %collective-permute-start.2) | collective-permute-done | bytes 2097184 | tf_op jit(solution)/shard_map/ppermute | solution.py:127
  446.4 3.1 constant_dynamic-update-slice_fusion
  449.6 1.5 fusion.5
  451.1 21.8 %all-gather.17.cloned.1.call-done = bf16[2048,2048]{1,0:T(8,128)(2,1)} async-done(((bf16[2048,512]{1,0:T(8,128)(2,1)}), bf16[2048,2048]{1,0:T(8,128)(2,1)}) %all-gather.17.cloned.1.call-update) | async-done | bytes 8388624 | tf_op jit(solution)/shard_map/all_gather | solution.py:154
  472.9 11.6 %convolution_convert_fusion.1 = bf16[256,2048]{1,0:T(8,128)(2,1)} fusion(bf16[2048,2048]{1,0:T(8,128)(2,1)} %all-gather.17.cloned.1.call-done, bf16[2048,2048]{1,0:T(8,128)(2,1)} %constant_dynamic-update-slice_fusion, bf16[256,2048]{1,0:T(8,128)(2,1)} %all-gather.15.cloned.1.call-done, f32[2048]{0:T(1024)S(1)} %copy-done.8, f32[256]{0:T(256)S(1)} %add_rsqrt_fusion), kind=kOutput, calls=%fused_computation.8 | convolution fusion | flops 4299161600 | bytes 18883584 | tf_op jit(solution)/shard_map/dot_general | solution.py:152
  484.5 24.7 %reduce-scatter.5.cloned.1.call-done = bf16[256,512]{1,0:T(8,128)(2,1)} async-done(((bf16[256,2048]{1,0:T(8,128)(2,1)}), bf16[256,512]{1,0:T(8,128)(2,1)}) %reduce-scatter.5.cloned.1.call-update) | async-done | bytes 262160 | tf_op jit(solution)/shard_map/reduce_scatter | solution.py:157
  509.2 1.7 add_convert_fusion
  (135 shorter events, 13.1 us)
Async XLA Ops:
  6.5 72.0 %copy-start = (bf16[4,128,128]{2,1,0:T(8,128)(2,1)S(1)}, bf16[4,128,128]{2,1,0:T(8,128)(2,1)}, u32[]{:S(2)}) copy-start(bf16[4,128,128]{2,1,0:T(8,128)(2,1)} %param.19) | copy-start | bytes 393220
  6.5 69.1 %copy-start.7 = (f32[2048]{0:T(1024)S(1)}, f32[2048]{0:T(1024)}, u32[]{:S(2)}) copy-start(f32[2048]{0:T(1024)} %param.14) | copy-start | bytes 24580
  6.5 21.8 %all-gather.7.cloned.1.call-start = ((), (), s32[]{:S(2)}) async-start(), calls=%async_computation.2 | async-start | bytes 1310720 | tf_op jit(solution)/shard_map/all_gather | solution.py:73
  7.3 68.3 %all-gather.9.cloned.1.call-start = ((), (), s32[]{:S(2)}) async-start(), calls=%async_computation.3 | async-start | bytes 2621440 | tf_op jit(solution)/shard_map/all_gather | solution.py:83
  8.0 113.7 %all-gather.11.cloned.1.call-start = ((), (), s32[]{:S(2)}) async-start(), calls=%async_computation.4 | async-start | bytes 2621440 | tf_op jit(solution)/shard_map/all_gather | solution.py:78
  8.7 158.9 %all-gather.13.cloned.1.call-start = ((), (), s32[]{:S(2)}) async-start(), calls=%async_computation.5 | async-start | bytes 2621440 | tf_op jit(solution)/shard_map/all_gather | solution.py:99
  9.3 186.9 %reduce-scatter.3.cloned.1.call-start = ((), (), s32[]{:S(2)}) async-start(), calls=%async_computation.6 | async-start | bytes 1310720 | tf_op jit(solution)/shard_map/reduce_scatter | solution.py:104
  78.3 0.9 copy-start.6
  78.9 0.8 copy-start.5
  84.9 82.7 %copy-start.4 = (bf16[256,2048]{1,0:T(8,128)(2,1)S(1)}, bf16[256,2048]{1,0:T(8,128)(2,1)}, u32[]{:S(2)}) copy-start(bf16[256,2048]{1,0:T(8,128)(2,1)} %all-gather.7.cloned.1.call-done) | copy-start | bytes 3145732
  85.2 111.0 %copy-start.3 = (bf16[256,512]{1,0:T(8,128)(2,1)S(1)}, bf16[256,512]{1,0:T(8,128)(2,1)}, u32[]{:S(2)}) copy-start(bf16[256,512]{1,0:T(8,128)(2,1)} %param.13) | copy-start | bytes 786436
  172.4 26.3 %copy-start.2 = (bf16[512,2048]{1,0:T(8,128)(2,1)S(1)}, bf16[512,2048]{1,0:T(8,128)(2,1)}, u32[]{:S(2)}) copy-start(bf16[512,2048]{1,0:T(8,128)(2,1)} %param.24) | copy-start | bytes 6291460
  172.4 277.2 %all-gather.15.cloned.1.call-start = ((), (), s32[]{:S(2)}) async-start(), calls=%async_computation.7 | async-start | bytes 1310720 | tf_op jit(solution)/shard_map/all_gather | solution.py:108
  197.9 275.0 %all-gather.17.cloned.1.call-start = ((), (), s32[]{:S(2)}) async-start(), calls=%async_computation.8 | async-start | bytes 10485760 | tf_op jit(solution)/shard_map/all_gather | solution.py:154
  198.7 310.5 %reduce-scatter.5.cloned.1.call-start = ((), (), s32[]{:S(2)}) async-start(), calls=%async_computation.9 | async-start | bytes 1310720 | tf_op jit(solution)/shard_map/reduce_scatter | solution.py:157
  198.7 69.2 %collective-permute-start = (bf16[512,2048]{1,0:T(8,128)(2,1)S(1)}, bf16[512,2048]{1,0:T(8,128)(2,1)}, u32[]{:S(2)}, u32[]{:S(2)}) collective-permute-start(bf16[512,2048]{1,0:T(8,128)(2,1)S(1)} %copy-done.2), channel_id=1, source_target_pairs={{0,4},{4,8},{8,12},{12,0},{1,5},{5,9},{9,13},{13,1},{2,6},{6,10},{... | collective-permute-start | bytes 6291464 | tf_op jit(solution)/shard_map/ppermute | solution.py:127
  200.3 207.3 %collective-permute-start.1 = (bf16[512,2048]{1,0:T(8,128)(2,1)S(1)}, bf16[512,2048]{1,0:T(8,128)(2,1)}, u32[]{:S(2)}, u32[]{:S(2)}) collective-permute-start(bf16[512,2048]{1,0:T(8,128)(2,1)S(1)} %copy-done.2), channel_id=1, source_target_pairs={{0,12},{4,0},{8,4},{12,8},{1,13},{5,1},{9,5},{13,9},{2,14},{6,2},{... | collective-permute-start | bytes 6291464 | tf_op jit(solution)/shard_map/ppermute | solution.py:136
  268.0 178.5 %collective-permute-start.2 = (bf16[512,2048]{1,0:T(8,128)(2,1)}, bf16[512,2048]{1,0:T(8,128)(2,1)}, u32[]{:S(2)}, u32[]{:S(2)}) collective-permute-start(bf16[512,2048]{1,0:T(8,128)(2,1)} %collective-permute-done), channel_id=1, source_target_pairs={{0,4},{4,8},{8,12},{12,0},{1,5},{5,9},{9,13},{13,1},{2,6},{6,10},{... | collective-permute-start | bytes 6291464 | tf_op jit(solution)/shard_map/ppermute | solution.py:127
  410.8 62.1 %copy-start.8 = (f32[2048]{0:T(1024)S(1)}, f32[2048]{0:T(1024)}, u32[]{:S(2)}) copy-start(f32[2048]{0:T(1024)} %param.15) | copy-start | bytes 24580
  451.1 58.1 %copy-start.1 = (bf16[256,512]{1,0:T(8,128)(2,1)S(1)}, bf16[256,512]{1,0:T(8,128)(2,1)}, u32[]{:S(2)}) copy-start(bf16[256,512]{1,0:T(8,128)(2,1)} %add_convert_fusion.1) | copy-start | bytes 786436
Sparse Core Ops, SparseCore 0:
  8.9 19.4 all-gather.6
  29.9 45.6 all-gather.8
  77.2 44.4 all-gather.10
  123.1 44.4 all-gather.12
  172.5 23.6 reduce-scatter.2
  198.0 16.6 all-gather.14
  216.4 256.4 all-gather.16
  484.6 24.4 reduce-scatter.4
